TPU v7x, 768 devices: a whole 4x8x12 slice. The times are simulated.
768 devices in a mesh: ep: 48 (over z, x), tp: 16 (over y, core).
Axes of the slice: x: 4, y: 8, z: 12, core: 2. Of those that a mesh axis runs over, the one named last changes fastest.
Arguments:
- tokens: bfloat16 [6144, 2048], P('ep'), may hold values from -6 to 6
- norm_gain: float32 [2048], replicated, may hold values from 0.1 to 1.9
- expert_ids: int32 [6144, 2], P('ep'), may hold values from 0 to 47, all different within a row; in each aligned block of 128 rows (0 to 127, 128 to 255, ...) at most 10 rows name the same one
- route_weights: float32 [6144, 2], P('ep'), may hold values from 0.2 to 1
- w_gate: bfloat16 [48, 2048, 4096], P('ep', None, 'tp'), may hold values from -0.125 to 0.125
- w_up: bfloat16 [48, 2048, 4096], P('ep', None, 'tp'), may hold values from -0.125 to 0.125
- w_down: bfloat16 [48, 4096, 2048], P('ep', 'tp'), may hold values from -0.09375 to 0.09375
Outputs:
- combined: bfloat16 [6144, 2048], P('ep', 'tp')
Inputs may be any that keep to these rules, and one draw needn't show every extreme that they name: `expert_ids`: each row names two different experts; among the rows of one device no expert is named more than 10 times, and in every draw some expert is named exactly 10 times there.
All inputs are finite; a program needn't handle non-finite values.
Results may differ from a plain program's by a relative error of at most 0.019.
Values may be sent and summed in bfloat16 or wider, within the bound.
A program may use at most 32 MiB of HBM per device.

v0:
```python
import jax
import jax.numpy as jnp
from jax import lax
from jax.sharding import PartitionSpec as P

epsilon = 1e-06


def in_order(blocks, dim):
    lengths = list(blocks.shape[1:])
    lengths[dim] *= blocks.shape[0]
    return jnp.moveaxis(blocks, 0, dim).reshape(lengths)


def from_everyone(x, axis):
    peers = lax.axis_size(axis)
    return lax.all_to_all(jnp.broadcast_to(x[None], (peers, *x.shape)), axis, 0, 0, tiled=True)


def gathered_copies(x, axis, dim):
    return in_order(from_everyone(x, axis), dim)


def split_up(x, dim, peers):
    lengths = x.shape
    blocks = x.reshape(*lengths[:dim], peers, lengths[dim] // peers, *lengths[dim + 1 :])
    return jnp.moveaxis(blocks, dim, 0)


def sent_and_summed(x, axis, dim):
    blocks = split_up(x, dim, lax.axis_size(axis))
    arrived = lax.all_to_all(blocks, axis, split_axis=0, concat_axis=0, tiled=True)
    return arrived.astype(jnp.float32).sum(axis=0)


def per_device(tokens, norm_gain, expert_ids, route_weights, w_gate, w_up, w_down):
    tok_rows, model_width = tokens.shape
    local_count = w_gate.shape[0]
    experts = local_count * lax.axis_size("ep")
    rank_count = lax.axis_size("tp")
    column_width = model_width // rank_count
    capacity = 4 * tok_rows // experts
    as_float = tokens.astype(jnp.float32)
    scale = lax.rsqrt(jnp.mean(as_float * as_float, axis=-1, keepdims=True) + epsilon)
    normed = (as_float * scale * norm_gain[None, :]).astype(jnp.bfloat16)
    flat_ids = expert_ids.reshape(-1)
    one_hot = (flat_ids[:, None] == jnp.arange(experts, dtype=jnp.int32)[None, :]).astype(jnp.int32)
    slot_index = jnp.sum((jnp.cumsum(one_hot, axis=0) - one_hot) * one_hot, axis=1)
    target = flat_ids * capacity + slot_index
    token_rows = jnp.repeat(normed, 2, axis=0)
    token_rows = lax.dynamic_slice_in_dim(
        token_rows, lax.axis_index("tp") * column_width, column_width, 1
    )
    outgoing = (
        jnp.zeros((experts * capacity, token_rows.shape[1]), jnp.bfloat16)
        .at[target]
        .set(token_rows)
    )
    outgoing = outgoing.reshape(experts, capacity, token_rows.shape[1])
    arrived = lax.all_to_all(outgoing, "ep", split_axis=0, concat_axis=1, tiled=True)
    piece = gathered_copies(arrived, "tp", 2)
    gate_part = jnp.einsum("erd,edf->erf", piece, w_gate, preferred_element_type=jnp.float32)
    up_part = jnp.einsum("erd,edf->erf", piece, w_up, preferred_element_type=jnp.float32)
    hidden = (jax.nn.silu(gate_part) * up_part).astype(jnp.bfloat16)
    partial_value = jnp.einsum("erf,efd->erd", hidden, w_down, preferred_element_type=jnp.float32)
    summed = sent_and_summed(partial_value.astype(jnp.bfloat16), "tp", 2).astype(jnp.bfloat16)
    returned = lax.all_to_all(summed, "ep", split_axis=1, concat_axis=0, tiled=True)
    picked = returned.reshape(experts * capacity, column_width)[target]
    picked = picked.reshape(tok_rows, 2, column_width).astype(jnp.float32)
    return jnp.sum(picked * route_weights[:, :, None], axis=1).astype(jnp.bfloat16)


def solution(mesh):
    in_specs = (
        P("ep", None),
        P(),
        P("ep", None),
        P("ep", None),
        P("ep", None, "tp"),
        P("ep", None, "tp"),
        P("ep", "tp", None),
    )
    out_specs = P("ep", "tp")
    return jax.shard_map(
        per_device, mesh=mesh, in_specs=in_specs, out_specs=out_specs, check_vma=False
    )
```

profile of v0, /device:TPU:1, one launch (start us, length us, event | category | flops | bytes accessed | tf_op | source)
XLA Modules:
  0.0 181.9 jit_solution(5195495760827855793)
XLA Ops:
  0.0 0.9 copy.22
  1.2 0.7 broadcast_multiply_fusion
  1.9 0.6 reduce-window.6
  3.0 1.2 fusion.13
  4.2 1.2 fusion.15
  5.4 0.6 broadcast_in_dim.9
  6.1 0.4 reshape.114
  6.6 1.2 scatter_custom_fusion
  7.9 32.6 %all_to_all.28 = bf16[48,10,128]{2,1,0:T(8,128)(2,1)S(1)} all-to-all(bf16[48,10,128]{2,1,0:T(8,128)(2,1)S(1)} %reshape.115), channel_id=1, replica_groups=mesh['ep'=48,'tp'=16] {'ep'}, dimensions={0} | all-to-all | bytes 245760 | tf_op jit(solution)/shard_map/all_to_all | solution.py:60
  40.8 57.8 %all_to_all.29 = bf16[16,1,480,128]{3,2,1,0:T(8,128)(2,1)S(1)} all-to-all(bf16[16,1,480,128]{3,2,1,0:T(8,128)(2,1)S(1)} %broadcast_in_dim.11), channel_id=1, replica_groups=mesh['ep'=48,'tp'=16] {'tp'}, dimensions={0} | all-to-all | bytes 3932160 | tf_op jit(solution)/shard_map/all_to_all | solution.py:17
  98.6 0.8 copy.25
  99.4 0.5 copy-done.2
  99.8 0.7 fusion.2
  100.5 4.7 %fusion.6 = bf16[60,8,16,128]{3,1,2,0:T(8,128)(2,1)} fusion(bf16[1,256,2048]{2,1,0:T(8,128)(2,1)S(1)} %copy-done, bf16[60,8,16,128]{3,2,1,0:T(8,128)(2,1)S(1)} %bitcast.68, bf16[1,2048,256]{2,1,0:T(8,128)(2,1)} %param.12, f32[480,256]{1,0:T(8,128)S(1)} %fusion.2), kind=kOutput, calls=%fused_computation.10 | convolution fusion | flops 1008353280 | bytes 6520832 | tf_op jit(solution)/shard_map/erf,efd->erd/dot_general | solution.py:65
  105.2 2.1 %copy.32 = bf16[60,8,16,128]{3,2,1,0:T(8,128)(2,1)S(1)} copy(bf16[60,8,16,128]{3,1,2,0:T(8,128)(2,1)} %fusion.6) | data formatting | bytes 3932160
  107.3 0.5 copy.51
  107.9 50.9 %all_to_all.30 = bf16[16,1,480,128]{3,2,1,0:T(8,128)(2,1)S(1)} all-to-all(bf16[16,1,480,128]{3,2,1,0:T(8,128)(2,1)S(1)} %bitcast.65), channel_id=1, replica_groups=mesh['ep'=48,'tp'=16] {'tp'}, dimensions={0} | all-to-all | bytes 3932160 | tf_op jit(solution)/shard_map/all_to_all | solution.py:32
  159.2 0.5 broadcast.75
  159.7 1.4 reduce.4
  161.1 0.7 reshape.142
  161.8 4.5 %all-to-all-start.3 = ((bf16[48,2,640]{2,1,0:T(2,128)(2,1)}), bf16[48,2,640]{2,1,0:T(2,128)(2,1)S(1)}, u32[]{:S(2)}, u32[]{:S(2)}) async-start(bf16[48,2,640]{2,1,0:T(2,128)(2,1)} %reshape.142), calls=%async_computation.3 | async-start | bytes 245760 | tf_op jit(solution)/shard_map/all_to_all | solution.py:67
  166.5 13.6 %all-to-all-done.3 = bf16[48,2,640]{2,1,0:T(2,128)(2,1)S(1)} async-done(((bf16[48,2,640]{2,1,0:T(2,128)(2,1)}), bf16[48,2,640]{2,1,0:T(2,128)(2,1)S(1)}, u32[]{:S(2)}, u32[]{:S(2)}) %all-to-all-start.3) | async-done | bytes 122912 | tf_op jit(solution)/shard_map/all_to_all | solution.py:67
  180.2 0.9 gather_fusion
  181.0 0.9 fusion.29
  (25 shorter events, 1.9 us)
Async XLA Ops:
  0.0 100.5 %copy-start = (bf16[1,256,2048]{2,1,0:T(8,128)(2,1)S(1)}, bf16[1,256,2048]{2,1,0:T(8,128)(2,1)}, u32[]{:S(2)}) copy-start(bf16[1,256,2048]{2,1,0:T(8,128)(2,1)} %param.13) | copy-start | bytes 3145732
  98.6 1.2 copy-start.2
  158.7 7.6 %copy-start.1 = (f32[128,2]{0,1:T(2,128)S(1)}, f32[128,2]{0,1:T(2,128)}, u32[]{:S(2)}) copy-start(f32[128,2]{0,1:T(2,128)} %param.10) | copy-start | bytes 3076
  161.8 18.2 %all-to-all-start.3 = ((bf16[48,2,640]{2,1,0:T(2,128)(2,1)}), bf16[48,2,640]{2,1,0:T(2,128)(2,1)S(1)}, u32[]{:S(2)}, u32[]{:S(2)}) async-start(bf16[48,2,640]{2,1,0:T(2,128)(2,1)} %reshape.142), calls=%async_computation.3 | async-start | bytes 245760 | tf_op jit(solution)/shard_map/all_to_all | solution.py:67
where the time goes:
time: 182 us
  blocking collectives  141 us (77%)
  waiting for transfers between devices  13.6 us (7%)
  local copies, waits for them, and re-layouts  10.5 us (6%)
  other arithmetic  6.43 us (4%)
  matrix products  5.37 us (3%)
  starting transfers between devices  4.52 us (2%)
    all_to_all x1, blocking collectives, from_everyone(): lax.all_to_all(jnp.broadcast_to(x[None], (peers, *x.shape)), axis, 0, 0,...  57.8 us
    all_to_all x1, blocking collectives, sent_and_summed(): lax.all_to_all(blocks, axis, split_axis=0, concat_axis=0, tiled=True)  50.9 us
    all_to_all x1, blocking collectives, per_device(): lax.all_to_all(outgoing, 'ep', split_axis=0, concat_axis=1, tiled=True)  32.6 us
    all_to_all x1, waiting for transfers between devices, per_device(): lax.all_to_all(summed, 'ep', split_axis=1, concat_axis=0, tiled=True)  13.6 us
    unnamed x13, local copies, waits for them, and re-layouts  4.88 us
    dot_general x1, matrix products, per_device(): jnp.einsum('erf,efd->erd', hidden, w_down, preferred_element_type=jnp.flo...  4.69 us
    all_to_all x1, starting transfers between devices, per_device(): lax.all_to_all(summed, 'ep', split_axis=1, concat_axis=0, tiled=True)  4.52 us
  transfers between devices with their start and end apart: 1, of which 1 were waited for; matrix products, arithmetic and copies ran while one was open for 0% of the time, Pallas kernels for 0%

commit v1 on v0

v1 whole, which is shorter than its diff:
```python
import functools

import jax
import jax.numpy as jnp
from jax import lax
from jax.experimental import pallas as pl
from jax.experimental.pallas import tpu as pltpu
from jax.sharding import PartitionSpec as P

MESH = pl.DeviceIdType.MESH
EPS = 1e-06
NX = 4
CHUNKS = 3
SKEW = 2


def z_offsets(nz):
    order = [0]
    for d in range(1, nz // 2 + 1):
        order.append(d)
        if d != nz - d:
            order.append(nz - d)
    return order


def kernel(
    sizes,
    tok_ref, gain_ref, ids_ref, rw_ref, wg_hbm, wu_hbm, wd_hbm,
    o_ref,
    wg, wu, wd, outg, X, own, psend, precv, rsend, rrecv, fo, ret, acc,
    w_sem, a2a_send, a2a_recv, gr_send, gr_recv, gp_send, gp_recv,
    rp_send, rp_recv, rr_send, rr_recv, ret_send, ret_recv,
):
    n_ep, ny, cap = sizes
    nz = n_ep // NX
    rows = n_ep * cap
    CR = rows // CHUNKS
    CB = n_ep // CHUNKS
    HP = cap // 2
    CP = CR // 2
    tok = tok_ref.shape[0]
    bf16, f32 = jnp.bfloat16, jnp.float32

    me = lax.axis_index("ep")
    t = lax.axis_index("tp")
    z, x = lax.div(me, NX), lax.rem(me, NX)
    y, c = lax.div(t, 2), lax.rem(t, 2)
    zs = z_offsets(nz)
    offsets = [(dz, dx) for dz in zs for dx in range(NX)]

    def ep_at(sign, p):
        dz, dx = offsets[p]
        return lax.rem(z + (nz + sign * dz) % nz, nz) * NX + lax.rem(x + (NX + sign * dx) % NX, NX)

    right = (me, lax.rem(y + 1, ny) * 2 + c)
    left = (me, lax.rem(y + ny - 1, ny) * 2 + c)
    partner = (me, y * 2 + 1 - c)

    barrier = pltpu.get_barrier_semaphore()
    for p in range(n_ep - 1, 0, -1):
        pl.semaphore_signal(barrier, inc=1, device_id=(ep_at(1, p), t), device_id_type=MESH)
    for peer in (left, right, partner):
        pl.semaphore_signal(barrier, inc=1, device_id=peer, device_id_type=MESH)

    w_copies = [
        pltpu.make_async_copy(src, dst, w_sem.at[i])
        for i, (src, dst) in enumerate(((wg_hbm, wg), (wu_hbm, wu), (wd_hbm, wd)))
    ]
    for copy in w_copies:
        copy.start()

    v = tok_ref[...].astype(f32)
    scale = lax.rsqrt(jnp.mean(v * v, axis=-1, keepdims=True) + EPS)
    mine = pl.ds(pl.multiple_of(t * 128, 128), 128)
    normed = (tok_ref[:, mine].astype(f32) * scale * gain_ref[:, mine]).astype(bf16)

    lanes = lax.broadcasted_iota(jnp.int32, (tok, 128), 1)
    ids = ids_ref[...]
    hit = [ids[:, k : k + 1] == lanes for k in range(2)]
    count = (hit[0] | hit[1]).astype(f32).astype(bf16)
    below = (
        lax.broadcasted_iota(jnp.int32, (tok, tok), 1) < lax.broadcasted_iota(jnp.int32, (tok, tok), 0)
    ).astype(f32).astype(bf16)
    earlier = jnp.dot(below, count, preferred_element_type=f32)
    target = []
    for k in range(2):
        slot = jnp.sum(jnp.where(hit[k], earlier, 0.0), axis=1, keepdims=True).astype(jnp.int32)
        e = ids[:, k : k + 1]
        dz = z - (e >> 2)
        dz = jnp.where(dz < 0, dz + nz, dz)
        dx = x - (e & 3)
        dx = jnp.where(dx < 0, dx + NX, dx)
        rank = jnp.where(dz * 2 <= nz, 2 * dz - 1, 2 * (nz - dz))
        rank = jnp.where(dz == 0, 0, rank)
        target.append((rank * NX + dx) * cap + slot)
    by_lane = [jnp.broadcast_to(a.astype(f32), (tok, tok)).T[0:1, :].astype(jnp.int32) for a in target]
    row = lax.broadcasted_iota(jnp.int32, (rows, tok), 0)
    select = ((row == by_lane[0]) | (row == by_lane[1])).astype(f32).astype(bf16)
    dispatch = jnp.dot(select, normed, preferred_element_type=f32).astype(bf16)
    outg.reshape(rows, 128)[...] = dispatch
    X[0, c, 0:HP] = dispatch[0:cap].reshape(HP, 2, 128)

    pl.semaphore_wait(barrier, n_ep + 2)

    def blocks(ref, p, n=1):
        return ref.at[pl.ds(p * HP, n * HP)]

    def remote(src, dst, ssem, rsem, dev):
        return pltpu.make_async_remote_copy(
            src_ref=src, dst_ref=dst, send_sem=ssem, recv_sem=rsem, device_id=dev, device_id_type=MESH
        )

    pending = []

    def go(*a):
        copy = remote(*a)
        copy.start()
        pending.append(copy)
        return copy

    for p in range(1, n_ep):
        remote(
            blocks(outg, p), blocks(X.at[0, c], p), a2a_send.at[0], a2a_recv.at[p // CB], (ep_at(-1, p), t)
        ).start()

    def pairs(j, lo=0, n=CP):
        return pl.ds(j * CP + lo, n)

    half = CP // 2

    def wait_gather(j, k, lo=0, n=CP, s=None):
        ref = X.at[k, c, pairs(j, lo, n)]
        remote(ref, ref, gr_send.at[j, 0], gr_recv.at[j, k if s is None else s], right).wait_recv()

    def to_partner(j, k):
        ref = X.at[k, c, pairs(j)]
        go(ref, ref, gp_send.at[j, k], gp_recv.at[j, k], partner)

    def forward(j, k, to_right, lo=0, n=CP, s=None):
        k2 = (k - 1) % ny if to_right else (k + 1) % ny
        s = k2 if s is None else s
        go(
            X.at[k, c, pairs(j, lo, n)], X.at[k2, c, pairs(j, lo, n)],
            gr_send.at[j, s], gr_recv.at[j, s], right if to_right else left,
        )

    far = ny // 2

    def gather_step(j, i):
        if i == 0:
            first = 1 if j == 0 else 0
            ref = blocks(X.at[0, c], j * CB + first, CB - first)
            remote(ref, ref, a2a_send.at[0], a2a_recv.at[j], right).wait_recv()
            forward(j, 0, True)
            forward(j, 0, False)
            to_partner(j, 0)
        elif i < far:
            wait_gather(j, ny - i)
            if i < far - 1:
                forward(j, ny - i, True)
            else:
                forward(j, ny - i, True, 0, half, far)
            wait_gather(j, i)
            if i < far - 1:
                forward(j, i, False)
            else:
                forward(j, i, False, half, CP - half, ny)
            to_partner(j, ny - i)
            to_partner(j, i)
        else:
            wait_gather(j, far, 0, half, far)
            wait_gather(j, far, half, CP - half, ny)
            to_partner(j, far)

    order = [far]
    for i in range(far - 1, 0, -1):
        order += [i, ny - i]
    order.append(0)

    def ffn(j):
        if j == 0:
            for copy in w_copies:
                copy.wait()
        gate = up = None
        for k in reversed(order):
            ref = X.at[k, 1 - c, pairs(j)]
            remote(ref, ref, gp_send.at[j, k], gp_recv.at[j, k], partner).wait_recv()
            lhs = jnp.concatenate(
                [X.at[k, q].reshape(rows, 128)[j * CR : (j + 1) * CR, :] for q in range(2)], axis=1
            )
            kk = pl.ds(pl.multiple_of(lax.rem(y + k, ny) * 256, 256), 256)
            dg = jnp.dot(lhs, wg[kk, :], preferred_element_type=f32)
            du = jnp.dot(lhs, wu[kk, :], preferred_element_type=f32)
            gate = dg if gate is None else gate + dg
            up = du if up is None else up + du
        hidden = (gate / (1.0 + jnp.exp(-gate)) * up).astype(bf16)
        for m in order:
            cols = pl.ds(pl.multiple_of(lax.rem(y + m, ny) * 256, 256), 256)
            part = jnp.dot(hidden, wd[:, cols], preferred_element_type=f32)
            lo, hi = part[:, :128], part[:, 128:]
            psend[j, m] = jnp.where(c == 0, hi, lo).astype(bf16)
            own[j, m] = jnp.where(c == 0, lo, hi)
            go(psend.at[j, m], precv.at[j, m], rp_send.at[j, m], rp_recv.at[j, m], partner)

    hr = CR // 2

    def both(j, m, lo, n):
        return own[j, m, lo : lo + n, :] + precv[j, m, lo : lo + n, :].astype(f32)

    def wait_pair(j, m):
        remote(psend.at[j, m], precv.at[j, m], rp_send.at[j, m], rp_recv.at[j, m], partner).wait_recv()

    def ring_wait(j, d, m, lo=0, n=CR):
        ref = rrecv.at[j, d, m, pl.ds(lo, n)]
        remote(ref, ref, rr_send.at[j, d, m], rr_recv.at[j, d, m], right).wait_recv()

    def ring_send(j, d, m, lo=0, n=CR):
        go(
            rsend.at[j, d, m, pl.ds(lo, n)], rrecv.at[j, d, m - 1, pl.ds(lo, n)],
            rr_send.at[j, d, m], rr_recv.at[j, d, m - 1], (right, left)[d],
        )

    def reduce_step(j, i):
        m = far - i
        if i == 0:
            wait_pair(j, far)
            for d, lo in ((0, 0), (1, hr)):
                rsend[j, d, m, lo : lo + hr, :] = both(j, far, lo, hr).astype(bf16)
                ring_send(j, d, m, lo, hr)
        elif i < far:
            for d in range(2):
                mine_m = m if d == 0 else ny - m
                wait_pair(j, mine_m)
                if i == 1:
                    lo = d * hr
                    other = hr - lo
                    rsend[j, d, m, other : other + hr, :] = both(j, mine_m, other, hr).astype(bf16)
                    ring_wait(j, d, m, lo, hr)
                    rsend[j, d, m, lo : lo + hr, :] = (
                        both(j, mine_m, lo, hr) + rrecv[j, d, m, lo : lo + hr, :].astype(f32)
                    ).astype(bf16)
                else:
                    ring_wait(j, d, m)
                    rsend[j, d, m] = (both(j, mine_m, 0, CR) + rrecv[j, d, m].astype(f32)).astype(bf16)
                ring_send(j, d, m)
        else:
            wait_pair(j, 0)
            total = both(j, 0, 0, CR)
            for d in range(2):
                ring_wait(j, d, 0)
                total = total + rrecv[j, d, 0].astype(f32)
            total = total.astype(bf16)
            fo.reshape(rows, 128)[j * CR : (j + 1) * CR, :] = total
            if j == 0:
                ret[0:HP] = total[0:cap].reshape(HP, 2, 128)
            for p in range(max(1, j * CB), (j + 1) * CB):
                remote(
                    blocks(fo, p), blocks(ret, p), ret_send.at[0], ret_recv.at[j], (ep_at(1, p), t)
                ).start()

    def combine(j):
        first = 1 if j == 0 else 0
        ref = blocks(ret, j * CB + first, CB - first)
        remote(ref, ref, ret_send.at[0], ret_recv.at[j], right).wait_recv()
        got = ret.reshape(rows, 128)[j * CR : (j + 1) * CR, :]
        place = lax.broadcasted_iota(jnp.int32, (tok, CR), 1) + j * CR
        total = None
        for k in range(2):
            pick = (place == target[k]).astype(f32).astype(bf16)
            value = jnp.dot(pick, got, preferred_element_type=f32) * rw_ref[:, k : k + 1]
            total = value if total is None else total + value
        if j == 0:
            acc[...] = total
        else:
            acc[...] += total

    stages = [functools.partial(gather_step, i=i) for i in range(far + 1)]
    stages.append(ffn)
    stages += [functools.partial(reduce_step, i=i) for i in range(far + 1)]
    for tick in range(len(stages) + SKEW * (CHUNKS - 1)):
        for j in range(CHUNKS):
            if 0 <= tick - SKEW * j < len(stages):
                stages[tick - SKEW * j](j)
    for j in range(CHUNKS):
        combine(j)
    o_ref[...] = acc[...].astype(bf16)

    ref = blocks(outg, 1, n_ep - 1)
    remote(ref, ref, a2a_send.at[0], a2a_recv.at[0], right).wait_send()
    ref = blocks(fo, 1, n_ep - 1)
    remote(ref, ref, ret_send.at[0], ret_recv.at[0], right).wait_send()
    for copy in pending:
        copy.wait_send()


def per_device(tokens, norm_gain, expert_ids, route_weights, w_gate, w_up, w_down):
    tok, width = tokens.shape
    n_ep, n_tp = lax.axis_size("ep"), lax.axis_size("tp")
    ny = n_tp // 2
    cap = 4 * tok // n_ep
    rows = n_ep * cap
    CR = rows // CHUNKS
    half = ny // 2
    bf16, f32 = jnp.bfloat16, jnp.float32
    vm = pl.BlockSpec(memory_space=pltpu.VMEM)
    hbm = pl.BlockSpec(memory_space=pl.ANY)
    dma = pltpu.SemaphoreType.DMA
    V = pltpu.VMEM
    ff = w_gate.shape[2]
    return pl.pallas_call(
        functools.partial(kernel, (n_ep, ny, cap)),
        out_shape=jax.ShapeDtypeStruct((tok, width // n_tp), bf16),
        in_specs=[vm, vm, vm, vm, hbm, hbm, hbm],
        out_specs=vm,
        scratch_shapes=[
            V((width, ff), bf16), V((width, ff), bf16), V((ff, width), bf16),
            V((rows // 2, 2, 128), bf16),
            V((ny, 2, rows // 2, 2, 128), bf16),
            V((CHUNKS, ny, CR, 128), f32),
            V((CHUNKS, ny, CR, 128), bf16),
            V((CHUNKS, ny, CR, 128), bf16),
            V((CHUNKS, 2, half + 1, CR, 128), bf16),
            V((CHUNKS, 2, half, CR, 128), bf16),
            V((rows // 2, 2, 128), bf16),
            V((rows // 2, 2, 128), bf16),
            V((tok, 128), f32),
            dma((3,)),
            dma((1,)), dma((CHUNKS,)),
            dma((CHUNKS, ny + 1)), dma((CHUNKS, ny + 1)),
            dma((CHUNKS, ny)), dma((CHUNKS, ny)),
            dma((CHUNKS, ny)), dma((CHUNKS, ny)),
            dma((CHUNKS, 2, half + 1)), dma((CHUNKS, 2, half)),
            dma((1,)), dma((CHUNKS,)),
        ],
        compiler_params=pltpu.CompilerParams(
            collective_id=0, has_side_effects=True, vmem_limit_bytes=48 * 1024 * 1024
        ),
        name="experts",
    )(
        tokens, norm_gain.reshape(1, width), expert_ids, route_weights, w_gate[0], w_up[0], w_down[0]
    )


def solution(mesh):
    in_specs = (
        P("ep", None),
        P(),
        P("ep", None),
        P("ep", None),
        P("ep", None, "tp"),
        P("ep", None, "tp"),
        P("ep", "tp", None),
    )
    return jax.shard_map(
        per_device, mesh=mesh, in_specs=in_specs, out_specs=P("ep", "tp"), check_vma=False
    )
```

time: 182 us -> 89.4 us (0.49)
  the two profiles are of different devices: /device:TPU:1 before, /device:TPU:8 now
where the time goes in v1:
time: 89.4 us; the launch traced here: 89.1 us
  Pallas kernels  81.7 us (91%)
  local copies, waits for them, and re-layouts  7.38 us (8%)
    pallas_call x1, Pallas kernels, per_device(): pl.pallas_call(functools.partial(kernel, (n_ep, ny, cap)), out_shape=jax....  81.7 us
    unnamed x17, local copies, waits for them, and re-layouts  7.38 us

profile of v1, /device:TPU:8, one launch (start us, length us, event | category | flops | bytes accessed | tf_op | source)
XLA Modules:
  0.0 89.1 jit_solution(16769784839104881305)
XLA Ops:
  0.0 0.0 copy-start.5
  0.0 0.7 copy-done.5
  0.7 0.0 copy-start.6
  0.7 0.1 copy.8.ids_ref
  0.8 0.6 copy-done.6
  1.4 0.0 copy-start.4
  1.4 0.1 copy.9.rw_ref
  1.5 0.6 copy-done.4
  2.1 0.0 copy-start
  2.1 1.2 %copy-done = bf16[1,2048,256]{2,1,0:T(8,128)(2,1)S(1)} copy-done((bf16[1,2048,256]{2,1,0:T(8,128)(2,1)S(1)}, bf16[1,2048,256]{2,1,0:T(8,128)(2,1)}, u32[]{:S(2)}) %copy-start) | copy-done | bytes 1048600
  3.3 0.0 copy-start.1
  3.3 1.2 %copy-done.1 = bf16[1,2048,256]{2,1,0:T(8,128)(2,1)S(1)} copy-done((bf16[1,2048,256]{2,1,0:T(8,128)(2,1)S(1)}, bf16[1,2048,256]{2,1,0:T(8,128)(2,1)}, u32[]{:S(2)}) %copy-start.1) | copy-done | bytes 1048600
  4.5 0.0 copy-start.2
  4.5 1.2 %copy-done.2 = bf16[1,256,2048]{2,1,0:T(8,128)(2,1)S(1)} copy-done((bf16[1,256,2048]{2,1,0:T(8,128)(2,1)S(1)}, bf16[1,256,2048]{2,1,0:T(8,128)(2,1)}, u32[]{:S(2)}) %copy-start.2) | copy-done | bytes 1048600
  5.7 0.0 copy-start.3
  5.7 1.0 %copy-done.3 = bf16[128,2048]{1,0:T(8,128)(2,1)S(1)} copy-done((bf16[128,2048]{1,0:T(8,128)(2,1)S(1)}, bf16[128,2048]{1,0:T(8,128)(2,1)}, u32[]{:S(2)}) %copy-start.3) | copy-done | bytes 524312
  6.8 81.7 %experts.1 = bf16[128,128]{1,0:T(8,128)(2,1)S(1)} custom-call(bf16[128,2048]{1,0:T(8,128)(2,1)S(1)} %copy-done.3, f32[1,2048]{1,0:T(1,128)S(1)} %bitcast.7, s32[128,2]{1,0:T(8,128)S(1)} %copy.8.ids_ref, f32[128,2]{1,0:T(8,128)S(1)} %copy.9.rw_ref, bf16[2048,256]{1,0:T(8,128)(2,1)S(1)} %bitcast.4, bf16[2048,256]{1,0:T(8,128)(2,1)S(1)} %bitcast.5, ...), custom_call_target="tpu_custom_call" | custom-call | tf_op jit(solution)/shard_map/experts/pallas_call | solution.py:310
  88.5 0.6 copy.11
Async XLA Ops:
  0.0 0.7 copy-start.5
  0.7 0.7 copy-start.6
  1.4 0.7 copy-start.4
  2.1 1.2 %copy-start = (bf16[1,2048,256]{2,1,0:T(8,128)(2,1)S(1)}, bf16[1,2048,256]{2,1,0:T(8,128)(2,1)}, u32[]{:S(2)}) copy-start(bf16[1,2048,256]{2,1,0:T(8,128)(2,1)} %param.11) | copy-start | bytes 3145732
  3.3 1.2 %copy-start.1 = (bf16[1,2048,256]{2,1,0:T(8,128)(2,1)S(1)}, bf16[1,2048,256]{2,1,0:T(8,128)(2,1)}, u32[]{:S(2)}) copy-start(bf16[1,2048,256]{2,1,0:T(8,128)(2,1)} %param.12) | copy-start | bytes 3145732
  4.5 1.2 %copy-start.2 = (bf16[1,256,2048]{2,1,0:T(8,128)(2,1)S(1)}, bf16[1,256,2048]{2,1,0:T(8,128)(2,1)}, u32[]{:S(2)}) copy-start(bf16[1,256,2048]{2,1,0:T(8,128)(2,1)} %param.13) | copy-start | bytes 3145732
  5.7 1.0 %copy-start.3 = (bf16[128,2048]{1,0:T(8,128)(2,1)S(1)}, bf16[128,2048]{1,0:T(8,128)(2,1)}, u32[]{:S(2)}) copy-start(bf16[128,2048]{1,0:T(8,128)(2,1)} %tok_ref.1) | copy-start | bytes 1572868
